TPU v7x, 512 devices: a 4x2x32 block of a 4x8x32 slice. The times are simulated.
512 devices in a mesh: grp: 2 (over y), fs: 32 (over z), tp: 8 (over x, core).
Axes of the slice: x: 4, y: 2, z: 32, core: 2. Of those that a mesh axis runs over, the one named last changes fastest.
The devices are a block of a 4x8x32 slice.
Arguments:
- tokens: bfloat16 [64, 384, 2048], P(('grp', 'fs'), None, 'tp'), parts along dimension 0, may hold values from -24 to 24
- input_gain: float32 [2048], replicated, may hold values from 0.1 to 1.9
- query_weight: bfloat16 [2048, 1024], P('fs', 'tp'), may hold values from -0.125 to 0.125
- key_weight: bfloat16 [2048, 1024], P('fs', 'tp'), may hold values from -0.125 to 0.125
- value_weight: bfloat16 [2048, 1024], P('fs', 'tp'), may hold values from -0.125 to 0.125
- output_gate_matrix: bfloat16 [2048, 1024], P('fs', 'tp'), may hold values from -0.125 to 0.125
- forward_decay: float32 [16], P('tp'), may hold values from -1 to 9
- backward_decay: float32 [16], P('tp'), may hold values from -1 to 9
- merge_weight: bfloat16 [1024, 2048], P('tp', 'fs'), may hold values from -0.375 to 0.375
- middle_gain: float32 [2048], replicated, may hold values from 0.1 to 1.9
- gate_weight: bfloat16 [2048, 5120], P('fs', 'tp'), may hold values from -0.125 to 0.125
- up_weight: bfloat16 [2048, 5120], P('fs', 'tp'), may hold values from -0.125 to 0.125
- down_weight: bfloat16 [5120, 2048], P('tp', 'fs'), may hold values from -0.15625 to 0.15625
Outputs:
- layer_out: bfloat16 [64, 384, 2048], P(('grp', 'fs'), None, 'tp'), parts along dimension 0
There are 2 independent parts, one for each index of `grp`. A program takes and returns all parts, laid end to end along the dimension named above; an argument that names none is the same for every part. Nothing has to cross between parts.
All inputs are finite; a program needn't handle non-finite values.
Results may differ from a plain program's by a relative error of at most 0.019.
Values may be sent and summed in bfloat16 or wider, within the bound.
No kernel may reach another device: no remote copies, remote signals or barrier semaphores. Data moves between devices by JAX's collectives and lax.ppermute only.
A program may use at most 64 MiB of HBM per device.

v0:
```python
import jax
import jax.numpy as jnp
from jax import lax
from jax.experimental import pallas as pl
from jax.experimental.pallas import tpu as pltpu
from jax.sharding import PartitionSpec as P


BLOCK = 128


norm_eps = 1e-06
group_eps = 1e-05
rope_base = 10000.0
highest_precision = lax.Precision.HIGHEST


def core_pairs():
    peers = lax.axis_size("tp")
    return [[i, i + 1] for i in range(0, peers, 2)]


def chip_rings():
    peers = lax.axis_size("tp")
    return [list(range(0, peers, 2)), list(range(1, peers, 2))]


def gathered_features(shard):
    chips = lax.all_gather(shard, "tp", axis=0, axis_index_groups=chip_rings())
    both = jnp.broadcast_to(chips, (2, *chips.shape))
    both = lax.all_to_all(both, "tp", 0, 0, tiled=True, axis_index_groups=core_pairs())
    return jnp.concatenate(
        [both[c, x] for x in range(chips.shape[0]) for c in range(2)], axis=1
    )


def by_core_and_chip(partial_term):
    peers = lax.axis_size("tp")
    width = partial_term.shape[1] // peers
    parts = [partial_term[:, t * width : (t + 1) * width] for t in range(peers)]
    return jnp.stack([jnp.stack(parts[0::2]), jnp.stack(parts[1::2])])


def scattered_sum(tiles):
    tiles = lax.all_to_all(tiles, "tp", 0, 0, tiled=True, axis_index_groups=core_pairs())
    return sum_over_chips(tiles[0], tiles[1])


def sum_over_chips(mine, theirs):
    chip_sum = (mine.astype(jnp.float32) + theirs.astype(jnp.float32)).astype(jnp.bfloat16)
    tiles = lax.all_to_all(chip_sum, "tp", 0, 0, tiled=True, axis_index_groups=chip_rings())
    return jnp.sum(tiles.astype(jnp.float32), axis=0)


def group_pairs():
    return [(i, i ^ 1) for i in range(lax.axis_size("grp"))]


def parity_rings():
    peers = lax.axis_size("fs")
    return [list(range(0, peers, 2)), list(range(1, peers, 2))]


def from_neighbours(ring):
    peers = lax.axis_size("fs")
    half = ring.shape[0] // 2
    upper = lax.ppermute(ring[:half], "fs", [(i, (i - 1) % peers) for i in range(peers)])
    lower = lax.ppermute(ring[half:], "fs", [(i, (i + 1) % peers) for i in range(peers)])
    return jnp.concatenate([upper, lower], axis=0)


def in_order(own, other, block):
    first = lax.axis_index("fs") % 2 == 0
    own = own.reshape(-1, block, own.shape[1])
    other = other.reshape(own.shape)
    both = jnp.stack([jnp.where(first, own, other), jnp.where(first, other, own)], axis=1)
    return both.reshape(-1, own.shape[2])


def gathered_by_pairs(left, right, common):
    paired = lax.axis_size("grp") % 2 == 0
    block, width = left.shape
    if not paired:
        rows = []
        for piece in (left, right, common):
            ring = lax.all_gather(piece, "fs", axis=0, tiled=True, axis_index_groups=parity_rings())
            rows.append(in_order(ring, from_neighbours(ring), block))
        return rows
    lower = lax.axis_index("grp") % 2 == 0
    mine = jnp.concatenate([jnp.where(lower, left, right), common], axis=1)
    ring = lax.all_gather(mine, "fs", axis=0, tiled=True, axis_index_groups=parity_rings())
    ring_pair = lax.ppermute(ring[:, :width], "grp", group_pairs())
    near = from_neighbours(ring)
    near_pair = from_neighbours(ring_pair)
    mine = in_order(ring, near, block)
    theirs = in_order(ring_pair, near_pair, block)
    return mine[:, :width], theirs, mine[:, width:]


def rms_scale(values, gain_vector):
    widened = values.astype(jnp.float32)
    scaled = widened * lax.rsqrt(jnp.mean(widened * widened, axis=-1, keepdims=True) + norm_eps)
    return (scaled * gain_vector).astype(jnp.bfloat16)


def apply_rotary_heads(values, length):
    half_dim = values.shape[-1] // 2
    inverse = rope_base ** (-jnp.arange(half_dim, dtype=jnp.float32) / half_dim)
    angles = jnp.arange(length, dtype=jnp.float32)[:, None] * inverse[None, :]
    cosine = jnp.cos(angles)[:, None, :]
    sine_part = jnp.sin(angles)[:, None, :]
    lower_half = values[..., :half_dim]
    upper_half = values[..., half_dim:]
    return jnp.concatenate(
        [
            lower_half * cosine - upper_half * sine_part,
            upper_half * cosine + lower_half * sine_part,
        ],
        axis=-1,
    )


def carry_states(key_blocks, value_blocks, weighting, log_rates, block_size, backward):
    block_terms = jnp.einsum(
        "sbmhd,sbmhe->bshde",
        key_blocks * weighting[None, None, :, :, None],
        value_blocks,
        precision=highest_precision,
    )
    factor = jnp.exp(log_rates * block_size)[None, :, None, None]

    def advance(running, addend):
        return (running * factor + addend, running)

    initial = jnp.zeros(block_terms.shape[1:], jnp.float32)
    return lax.scan(advance, initial, block_terms, reverse=backward)[1]


def retain_blocks(
    query_rows, key_rows, value_rows, gate_rows, forward_decay, backward_decay, seq_count, length
):
    head_count = forward_decay.shape[0]
    head_dim = query_rows.shape[1] // head_count
    block_size = BLOCK
    block_count = length // block_size

    def split_heads(rows_in):
        return rows_in.astype(jnp.float32).reshape(seq_count, length, head_count, head_dim)

    def blocked(tensor):
        return tensor.reshape(seq_count, block_count, block_size, head_count, head_dim)

    queries = blocked(apply_rotary_heads(split_heads(query_rows), length))
    key_heads = blocked(apply_rotary_heads(split_heads(key_rows), length) * head_dim ** (-0.5))
    valued = blocked(split_heads(value_rows))
    rate_ahead = jax.nn.log_sigmoid(forward_decay)
    rate_behind = jax.nn.log_sigmoid(backward_decay)
    position = jnp.arange(block_size, dtype=jnp.float32)
    offset = position[:, None] - position[None, :]
    inside = jnp.where(
        offset[None] >= 0,
        jnp.exp(rate_ahead[:, None, None] * jnp.maximum(offset, 0.0)[None]),
        jnp.exp(rate_behind[:, None, None] * jnp.maximum(-offset, 0.0)[None]),
    )
    attention_scores = (
        jnp.einsum("sbchd,sbmhd->sbhcm", queries, key_heads, precision=highest_precision)
        * inside[None, None]
    )
    result = jnp.einsum("sbhcm,sbmhd->sbchd", attention_scores, valued, precision=highest_precision)
    column = position[:, None]
    key_ahead = jnp.exp(rate_ahead[None, :] * (block_size - 1 - column))
    query_ahead = jnp.exp(rate_ahead[None, :] * (column + 1))
    key_behind = jnp.exp(rate_behind[None, :] * column)
    query_behind = jnp.exp(rate_behind[None, :] * (block_size - column))
    from_before = carry_states(key_heads, valued, key_ahead, rate_ahead, block_size, False)
    from_after = carry_states(key_heads, valued, key_behind, rate_behind, block_size, True)
    result = (
        result
        + jnp.einsum("sbchd,bshde->sbche", queries, from_before, precision=highest_precision)
        * query_ahead[None, None, :, :, None]
    )
    result = (
        result
        + jnp.einsum("sbchd,bshde->sbche", queries, from_after, precision=highest_precision)
        * query_behind[None, None, :, :, None]
    )
    result = result.reshape(seq_count, length, head_count, head_dim)
    center = jnp.mean(result, axis=-1, keepdims=True)
    spread = jnp.mean(jnp.square(result - center), axis=-1, keepdims=True)
    normalized = (result - center) * lax.rsqrt(spread + group_eps)
    gated = jax.nn.silu(split_heads(gate_rows)) * normalized
    return gated.reshape(seq_count * length, head_count * head_dim).astype(jnp.bfloat16)


def down_share(hidden_ref, weights):
    return lax.dot_general(
        hidden_ref[...], weights, (((1,), (1,)), ((), ())), preferred_element_type=jnp.float32
    ).astype(jnp.bfloat16)


def feed_forward_kernel(
    core_ref,
    normed_ref,
    packed_ref,
    other_ref,
    hidden_ref,
    own_down_ref,
    upper_ref,
    down_ref,
    acts_ref,
    upper_sem,
    down_sem,
    own_sem,
):
    units = hidden_ref.shape[1]
    blocks, depth = upper_ref.shape[0], upper_ref.shape[1]
    chips, width = down_ref.shape[0], down_ref.shape[1]
    core = core_ref[0]
    upper, down, own = [], [], []
    for k in range(blocks):
        source = packed_ref.at[pl.ds(k * depth, depth), pl.ds(0, 2 * units)]
        upper.append(pltpu.make_async_copy(source, upper_ref.at[k], upper_sem.at[k]))
    for chip in range(chips):
        rows = pl.ds((2 * chip + 1 - core) * width, width)
        source = packed_ref.at[rows, pl.ds(2 * units, units)]
        down.append(pltpu.make_async_copy(source, down_ref.at[chip], down_sem.at[chip]))
    for chip in range(chips):
        rows = pl.ds((2 * chip + core) * width, width)
        source = packed_ref.at[rows, pl.ds(2 * units, units)]
        own.append(pltpu.make_async_copy(source, own_down_ref.at[chip], own_sem.at[chip]))
    for copy in upper + down + own:
        copy.start()
    for k in range(blocks):
        upper[k].wait()
        term = jnp.dot(
            normed_ref[:, k * depth : (k + 1) * depth],
            upper_ref[k],
            preferred_element_type=jnp.float32,
        )
        if k == 0:
            acts_ref[...] = term
        else:
            acts_ref[...] += term
    gate_act, up_act = acts_ref[:, :units], acts_ref[:, units:]
    hidden = gate_act / (1.0 + jnp.exp(-gate_act)) * up_act
    hidden_ref[...] = hidden.astype(hidden_ref.dtype)
    for copy in down + own:
        copy.wait()
    for chip in range(chips):
        other_ref[chip] = down_share(hidden_ref, down_ref[chip])


def own_share_kernel(hidden_ref, own_down_ref, own_ref):
    for chip in range(own_ref.shape[0]):
        own_ref[chip] = down_share(hidden_ref, own_down_ref[chip])


def feed_forward(normed_mid, packed, core, peers):
    rows, features = normed_mid.shape
    units = packed.shape[1] // 3
    chips, width, depth = peers // 2, features // peers, 512
    blocks = features // depth
    vmem = pl.BlockSpec(memory_space=pltpu.VMEM)
    return pl.pallas_call(
        feed_forward_kernel,
        out_shape=[
            jax.ShapeDtypeStruct((chips, rows, width), jnp.bfloat16),
            jax.ShapeDtypeStruct((rows, units), jnp.bfloat16),
            jax.ShapeDtypeStruct((chips, width, units), jnp.bfloat16),
        ],
        in_specs=[
            pl.BlockSpec(memory_space=pltpu.SMEM),
            vmem,
            pl.BlockSpec(memory_space=pltpu.HBM),
        ],
        out_specs=[vmem, vmem, vmem],
        scratch_shapes=[
            pltpu.VMEM((blocks, depth, 2 * units), jnp.bfloat16),
            pltpu.VMEM((chips, width, units), jnp.bfloat16),
            pltpu.VMEM((rows, 2 * units), jnp.float32),
            pltpu.SemaphoreType.DMA((blocks,)),
            pltpu.SemaphoreType.DMA((chips,)),
            pltpu.SemaphoreType.DMA((chips,)),
        ],
        compiler_params=pltpu.CompilerParams(vmem_limit_bytes=48 * 1024 * 1024),
    )(core, normed_mid, packed)


def own_share(hidden, own_down):
    chips, width, _ = own_down.shape
    vmem = pl.BlockSpec(memory_space=pltpu.VMEM)
    return pl.pallas_call(
        own_share_kernel,
        out_shape=jax.ShapeDtypeStruct((chips, hidden.shape[0], width), jnp.bfloat16),
        in_specs=[vmem, vmem],
        out_specs=vmem,
        compiler_params=pltpu.CompilerParams(vmem_limit_bytes=8 * 1024 * 1024),
    )(hidden, own_down)


def on_device(
    tokens,
    input_gain,
    query_weight,
    key_weight,
    value_weight,
    output_gate_matrix,
    forward_decay,
    backward_decay,
    merge_weight,
    middle_gain,
    gate_weight,
    up_weight,
    down_weight,
):
    seq_count, length, part_width = tokens.shape
    row_count = seq_count * length
    packed = jnp.concatenate([gate_weight, up_weight, down_weight.T], axis=1)
    packed = lax.all_gather(packed, "fs", axis=0, tiled=True)

    mine_full, theirs_full, merge_full = gathered_by_pairs(
        jnp.concatenate([query_weight, key_weight], axis=1),
        jnp.concatenate([value_weight, output_gate_matrix], axis=1),
        merge_weight.T,
    )
    local = tokens.reshape(row_count, part_width)
    normed = rms_scale(gathered_features(local), input_gain)

    def project(weight):
        return jnp.dot(normed, weight, preferred_element_type=jnp.float32).astype(jnp.bfloat16)

    mine_rows, theirs_rows = project(mine_full), project(theirs_full)
    lower = lax.axis_index("grp") % 2 == 0
    lower = jnp.logical_or(lower, lax.axis_size("grp") % 2 == 1)
    left_rows = jnp.where(lower, mine_rows, theirs_rows)
    right_rows = jnp.where(lower, theirs_rows, mine_rows)
    head_width = query_weight.shape[1]
    mixed = retain_blocks(
        left_rows[:, :head_width],
        left_rows[:, head_width:],
        right_rows[:, :head_width],
        right_rows[:, head_width:],
        forward_decay,
        backward_decay,
        seq_count,
        length,
    )
    merge_term = jnp.einsum("rh,dh->rd", mixed, merge_full, preferred_element_type=jnp.float32)
    merged = scattered_sum(by_core_and_chip(merge_term.astype(jnp.bfloat16)))
    middle = (local.astype(jnp.float32) + merged).astype(jnp.bfloat16)
    normed_mid = rms_scale(gathered_features(middle), middle_gain)
    peers = lax.axis_size("tp")
    core = (lax.axis_index("tp") % 2).astype(jnp.int32).reshape(1)
    other, hidden, own_down = feed_forward(normed_mid, packed, core, peers)
    theirs = lax.ppermute(other, "tp", [(i, i ^ 1) for i in range(peers)])
    mine = own_share(hidden, own_down)
    summed = sum_over_chips(mine, theirs)
    layer_out = (middle.astype(jnp.float32) + summed).astype(jnp.bfloat16)
    return layer_out.reshape(seq_count, length, part_width)


def solution(mesh):
    placed = (
        P(("grp", "fs"), None, "tp"),
        P(),
        P("fs", "tp"),
        P("fs", "tp"),
        P("fs", "tp"),
        P("fs", "tp"),
        P("tp"),
        P("tp"),
        P("tp", "fs"),
        P(),
        P("fs", "tp"),
        P("fs", "tp"),
        P("tp", "fs"),
    )

    return jax.shard_map(
        on_device,
        mesh=mesh,
        in_specs=placed,
        out_specs=P(("grp", "fs"), None, "tp"),
        check_vma=False,
    )
```

profile of v0, /device:TPU:33, one launch (start us, length us, event | category | flops | bytes accessed | tf_op | source)
XLA Modules:
  0.0 295.2 jit_solution(1431393854413619317)
XLA Ops:
  6.5 0.8 maximum_select_fusion
  7.4 0.7 pad_maximum_fusion.5
  8.1 74.5 %all_gather.14 = bf16[1024,384]{1,0:T(8,128)(2,1)S(1)} all-gather(bf16[64,384]{1,0:T(8,128)(2,1)S(1)} %pad_maximum_fusion.5), channel_id=1, replica_groups={{0,16,32,48,64,80,96,112,128,144,160,176,192,208,224,240},{8,24,40,56,7..., dimensions={0}, use_global_device_ids=true | all-gather | bytes 835584 | tf_op jit(solution)/shard_map/all_gather | solution.py:91
  82.6 1.0 fusion.63
  83.5 3.5 %collective-permute-start.3 = (bf16[512,384]{1,0:T(8,128)(2,1)}, bf16[512,384]{1,0:T(8,128)(2,1)}, u32[]{:S(2)}, u32[]{:S(2)}) collective-permute-start(bf16[512,384]{1,0:T(8,128)(2,1)} %get-tuple-element.256), channel_id=1, source_target_pairs={{0,248},{8,0},{16,8},{24,16},{32,24},{40,32},{48,40},{56,48},{64,5... | collective-permute-start | bytes 1179656 | tf_op jit(solution)/shard_map/ppermute | solution.py:67
  87.0 2.0 collective-permute-start.4
  89.0 10.9 %all_gather.13 = bf16[4,384,256]{2,1,0:T(8,128)(2,1)S(1)} all-gather(bf16[1,384,256]{2,1,0:T(8,128)(2,1)S(1)} %copy-done.2), channel_id=1, replica_groups={{0,2,4,6},{1,3,5,7},{8,10,12,14},{9,11,13,15},{16,18,20,22},{17,19,21,2..., dimensions={0}, use_global_device_ids=true | all-gather | bytes 983040 | tf_op jit(solution)/shard_map/all_gather | solution.py:29
  99.9 1.4 broadcast_in_dim.28
  101.2 15.4 %all-to-all-start = ((bf16[2,4,384,256]{3,2,1,0:T(8,128)(2,1)}), bf16[2,4,384,256]{3,2,1,0:T(8,128)(2,1)S(1)}, u32[]{:S(2)}, u32[]{:S(2)}) async-start(bf16[2,4,384,256]{3,2,1,0:T(8,128)(2,1)} %broadcast_in_dim.28), calls=%async_computation | async-start | bytes 3145728 | tf_op jit(solution)/shard_map/all_to_all | solution.py:31
  116.6 0.8 slice.172
  117.4 3.5 %collective-permute-start = (bf16[1024,256]{1,0:T(8,128)(2,1)}, bf16[1024,256]{1,0:T(8,128)(2,1)S(1)}, u32[]{:S(2)}, u32[]{:S(2)}) collective-permute-start(bf16[1024,256]{1,0:T(8,128)(2,1)} %slice.172), channel_id=1, source_target_pairs={{0,256},{256,0},{1,257},{257,1},{2,258},{258,2},{3,259},{259,3},{4... | collective-permute-start | bytes 1572872 | tf_op jit(solution)/shard_map/ppermute | solution.py:92
  121.0 0.7 pad_maximum_fusion.3
  122.1 1.2 copy-done
  123.3 0.4 fusion
  123.8 0.7 multiply_exponential_fusion
  124.4 0.6 multiply_exponential_fusion.1
  125.0 0.9 fusion.53
  126.2 1.0 constant_dynamic-update-slice_fusion.3
  127.2 1.1 constant_dynamic-update-slice_fusion.2
  128.6 4.6 %collective-permute-done = bf16[1024,256]{1,0:T(8,128)(2,1)S(1)} collective-permute-done((bf16[1024,256]{1,0:T(8,128)(2,1)}, bf16[1024,256]{1,0:T(8,128)(2,1)S(1)}, u32[]{:S(2)}, u32[]{:S(2)}) %collective-permute-start) | collective-permute-done | bytes 524320 | tf_op jit(solution)/shard_map/ppermute | solution.py:92
  133.3 3.1 %collective-permute-start.1 = (bf16[512,256]{1,0:T(8,128)(2,1)S(1)}, bf16[512,256]{1,0:T(8,128)(2,1)S(1)}, u32[]{:S(2)}, u32[]{:S(2)}) collective-permute-start(bf16[512,256]{1,0:T(8,128)(2,1)S(1)} %get-tuple-element.258), channel_id=1, source_target_pairs={{0,248},{8,0},{16,8},{24,16},{32,24},{40,32},{48,40},{56,48},{64,5... | collective-permute-start | bytes 786440 | tf_op jit(solution)/shard_map/ppermute | solution.py:67
  136.4 2.5 collective-permute-start.2
  139.0 0.9 convolution_convert_fusion.1
  139.9 7.5 %collective-permute-done.1 = bf16[512,256]{1,0:T(8,128)(2,1)S(1)} collective-permute-done((bf16[512,256]{1,0:T(8,128)(2,1)S(1)}, bf16[512,256]{1,0:T(8,128)(2,1)S(1)}, u32[]{:S(2)}, u32[]{:S(2)}) %collective-permute-start.1) | collective-permute-done | bytes 262176 | tf_op jit(solution)/shard_map/ppermute | solution.py:67
  147.4 4.9 %collective-permute-done.2 = bf16[512,256]{1,0:T(8,128)(2,1)S(1)} collective-permute-done((bf16[512,256]{1,0:T(8,128)(2,1)S(1)}, bf16[512,256]{1,0:T(8,128)(2,1)S(1)}, u32[]{:S(2)}, u32[]{:S(2)}) %collective-permute-start.2) | collective-permute-done | bytes 262176 | tf_op jit(solution)/shard_map/ppermute | solution.py:68
  152.5 0.6 copy-done.11
  153.1 0.9 broadcast_select_fusion.5
  154.9 0.9 convolution_bitcast_fusion.3
  156.2 0.5 fusion.8
  157.0 0.5 fusion.9
  157.5 0.8 convolution_multiply_fusion
  158.3 0.5 fusion.66
  159.1 0.6 convolution_convert_fusion
  160.2 7.0 %all_to_all.25 = bf16[2,4,384,256]{3,2,1,0:T(8,128)(2,1)S(1)} all-to-all(bf16[2,4,384,256]{3,2,1,0:T(8,128)(2,1)S(1)} %pad_maximum_fusion.1), channel_id=1, replica_groups={{0,1},{2,3},{4,5},{6,7},{8,9},{10,11},{12,13},{14,15},{16,17},{18,19},{..., dimensions={0} | all-to-all | bytes 3145728 | tf_op jit(solution)/shard_map/all_to_all | solution.py:45
  167.2 1.1 fusion.11
  168.3 3.6 %all-to-all-start.2 = ((bf16[4,384,256]{2,1,0:T(8,128)(2,1)}), bf16[4,384,256]{2,1,0:T(8,128)(2,1)S(1)}, u32[]{:S(2)}, u32[]{:S(2)}) async-start(bf16[4,384,256]{2,1,0:T(8,128)(2,1)} %fusion.11), calls=%async_computation.2 | async-start | bytes 1572864 | tf_op jit(solution)/shard_map/all_to_all | solution.py:51
  171.9 11.7 %all-to-all-done.2 = bf16[4,384,256]{2,1,0:T(8,128)(2,1)S(1)} async-done(((bf16[4,384,256]{2,1,0:T(8,128)(2,1)}), bf16[4,384,256]{2,1,0:T(8,128)(2,1)S(1)}, u32[]{:S(2)}, u32[]{:S(2)}) %all-to-all-start.2) | async-done | bytes 786464 | tf_op jit(solution)/shard_map/all_to_all | solution.py:51
  183.8 11.2 %all_gather.15 = bf16[4,384,256]{2,1,0:T(8,128)(2,1)S(1)} all-gather(bf16[1,384,256]{2,1,0:T(8,128)(2,1)S(1)} %fusion.16), channel_id=1, replica_groups={{0,2,4,6},{1,3,5,7},{8,10,12,14},{9,11,13,15},{16,18,20,22},{17,19,21,2..., dimensions={0}, use_global_device_ids=true | all-gather | bytes 983040 | tf_op jit(solution)/shard_map/all_gather | solution.py:29
  195.1 9.1 %all_to_all.26 = bf16[2,4,384,256]{3,2,1,0:T(8,128)(2,1)S(1)} all-to-all(bf16[2,4,384,256]{3,2,1,0:T(8,128)(2,1)S(1)} %broadcast_in_dim.33), channel_id=1, replica_groups={{0,1},{2,3},{4,5},{6,7},{8,9},{10,11},{12,13},{14,15},{16,17},{18,19},{..., dimensions={0} | all-to-all | bytes 3145728 | tf_op jit(solution)/shard_map/all_to_all | solution.py:31
  204.5 0.4 fusion.3
  205.1 0.4 fusion.5.normed_ref
  205.5 37.4 %all-gather.2.cloned.1.call-done.packed_ref = bf16[2048,1920]{1,0:T(8,128)(2,1)} async-done(((bf16[64,1920]{1,0:T(8,128)(2,1)}), bf16[2048,1920]{1,0:T(8,128)(2,1)}) %all-gather.2.cloned.1.call-update) | async-done | bytes 7864336 | tf_op jit(solution)/shard_map/all_gather | solution.py:319
  242.9 5.3 %shard_map.127 = (bf16[4,384,256]{2,1,0:T(8,128)(2,1)S(1)}, bf16[384,640]{1,0:T(8,128)(2,1)S(1)}, bf16[4,256,640]{2,1,0:T(8,128)(2,1)S(1)}) custom-call(s32[1]{0:T(128)} %bitcast.49.core_ref, bf16[384,2048]{1,0:T(8,128)(2,1)S(1)} %fusion.5.normed_ref, bf16[2048,1920]{1,0:T(8,128)(2,1)} %all-gather.2.cloned.1.call-done.packed_ref), custom_call_target="tpu_custom_call" | custom-call | tf_op jit(solution)/shard_map/pallas_call | solution.py:264
  248.2 21.5 %collective-permute-start.5 = (bf16[4,384,256]{2,1,0:T(8,128)(2,1)S(1)}, bf16[4,384,256]{2,1,0:T(8,128)(2,1)S(1)}, u32[]{:S(2)}, u32[]{:S(2)}) collective-permute-start(bf16[4,384,256]{2,1,0:T(8,128)(2,1)S(1)} %get-tuple-element.142), channel_id=1, source_target_pairs={{0,1},{1,0},{2,3},{3,2},{4,5},{5,4},{6,7},{7,6},{8,9},{9,8},{10,11... | collective-permute-start | bytes 2359304 | tf_op jit(solution)/shard_map/ppermute | solution.py:355
  269.7 0.8 shard_map.128
  270.5 1.1 collective-permute-done.5
  271.8 15.8 %all_to_all.27 = bf16[4,384,256]{2,1,0:T(8,128)(2,1)S(1)} all-to-all(bf16[4,384,256]{2,1,0:T(8,128)(2,1)S(1)} %add_convert_fusion), channel_id=1, replica_groups={{0,2,4,6},{1,3,5,7},{8,10,12,14},{9,11,13,15},{16,18,20,22},{17,19,21,2..., dimensions={0} | all-to-all | bytes 1572864 | tf_op jit(solution)/shard_map/all_to_all | solution.py:51
  287.6 0.7 fusion.15
  (110 shorter events, 4.7 us)
Async XLA Ops:
  6.5 82.4 %copy-start.2 = (bf16[1,384,256]{2,1,0:T(8,128)(2,1)S(1)}, bf16[1,384,256]{2,1,0:T(8,128)(2,1)}, u32[]{:S(2)}) copy-start(bf16[1,384,256]{2,1,0:T(8,128)(2,1)} %param.17) | copy-start | bytes 589828
  83.5 42.6 %collective-permute-start.3 = (bf16[512,384]{1,0:T(8,128)(2,1)}, bf16[512,384]{1,0:T(8,128)(2,1)}, u32[]{:S(2)}, u32[]{:S(2)}) collective-permute-start(bf16[512,384]{1,0:T(8,128)(2,1)} %get-tuple-element.256), channel_id=1, source_target_pairs={{0,248},{8,0},{16,8},{24,16},{32,24},{40,32},{48,40},{56,48},{64,5... | collective-permute-start | bytes 1179656 | tf_op jit(solution)/shard_map/ppermute | solution.py:67
  87.0 40.2 %collective-permute-start.4 = (bf16[512,384]{1,0:T(8,128)(2,1)}, bf16[512,384]{1,0:T(8,128)(2,1)}, u32[]{:S(2)}, u32[]{:S(2)}) collective-permute-start(bf16[512,384]{1,0:T(8,128)(2,1)} %get-tuple-element.255), channel_id=1, source_target_pairs={{0,8},{8,16},{16,24},{24,32},{32,40},{40,48},{48,56},{56,64},{64,7... | collective-permute-start | bytes 1179656 | tf_op jit(solution)/shard_map/ppermute | solution.py:68
  101.2 19.8 %copy-start.5 = (bf16[640,64]{0,1:T(8,128)(2,1)S(1)}, bf16[640,64]{0,1:T(8,128)(2,1)}, u32[]{:S(2)}) copy-start(bf16[640,64]{0,1:T(8,128)(2,1)} %param.29) | copy-start | bytes 245764
  101.2 19.8 %copy-start.6 = (bf16[64,640]{1,0:T(8,128)(2,1)S(1)}, bf16[64,640]{1,0:T(8,128)(2,1)}, u32[]{:S(2)}) copy-start(bf16[64,640]{1,0:T(8,128)(2,1)} %param.28) | copy-start | bytes 245764
  101.2 19.8 %copy-start.7 = (bf16[64,640]{1,0:T(8,128)(2,1)S(1)}, bf16[64,640]{1,0:T(8,128)(2,1)}, u32[]{:S(2)}) copy-start(bf16[64,640]{1,0:T(8,128)(2,1)} %param.27) | copy-start | bytes 245764
  101.2 20.6 %all-to-all-start = ((bf16[2,4,384,256]{3,2,1,0:T(8,128)(2,1)}), bf16[2,4,384,256]{3,2,1,0:T(8,128)(2,1)S(1)}, u32[]{:S(2)}, u32[]{:S(2)}) async-start(bf16[2,4,384,256]{3,2,1,0:T(8,128)(2,1)} %broadcast_in_dim.28), calls=%async_computation | async-start | bytes 3145728 | tf_op jit(solution)/shard_map/all_to_all | solution.py:31
  116.6 126.3 %all-gather.2.cloned.1.call-start = ((), (), s32[]{:S(2)}) async-start(), calls=%async_computation.5 | async-start | bytes 8110080 | tf_op jit(solution)/shard_map/all_gather | solution.py:319
  117.4 15.8 %collective-permute-start = (bf16[1024,256]{1,0:T(8,128)(2,1)}, bf16[1024,256]{1,0:T(8,128)(2,1)S(1)}, u32[]{:S(2)}, u32[]{:S(2)}) collective-permute-start(bf16[1024,256]{1,0:T(8,128)(2,1)} %slice.172), channel_id=1, source_target_pairs={{0,256},{256,0},{1,257},{257,1},{2,258},{258,2},{3,259},{259,3},{4... | collective-permute-start | bytes 1572872 | tf_op jit(solution)/shard_map/ppermute | solution.py:92
  121.9 1.8 copy-start.12
  122.0 1.8 copy-start.13
  122.1 1.3 copy-start
  125.0 13.9 %copy-start.10 = (f32[384]{0:T(512)}, f32[384]{0:T(512)S(1)}, u32[]{:S(2)}) copy-start(f32[384]{0:T(512)S(1)} %add_rsqrt_fusion.1) | copy-start | bytes 4612
  128.4 10.5 %copy-start.1 = (bf16[384,2048]{1,0:T(8,128)(2,1)S(1)}, bf16[384,2048]{1,0:T(8,128)(2,1)}, u32[]{:S(2)}) copy-start(bf16[384,2048]{1,0:T(8,128)(2,1)} %copy-done) | copy-start | bytes 4718596
  128.4 10.5 %copy-start.14 = (f32[2048]{0:T(1024)S(1)}, f32[2048]{0:T(1024)}, u32[]{:S(2)}) copy-start(f32[2048]{0:T(1024)} %param.18) | copy-start | bytes 24580
  133.3 14.0 %collective-permute-start.1 = (bf16[512,256]{1,0:T(8,128)(2,1)S(1)}, bf16[512,256]{1,0:T(8,128)(2,1)S(1)}, u32[]{:S(2)}, u32[]{:S(2)}) collective-permute-start(bf16[512,256]{1,0:T(8,128)(2,1)S(1)} %get-tuple-element.258), channel_id=1, source_target_pairs={{0,248},{8,0},{16,8},{24,16},{32,24},{40,32},{48,40},{56,48},{64,5... | collective-permute-start | bytes 786440 | tf_op jit(solution)/shard_map/ppermute | solution.py:67
  136.4 15.8 %collective-permute-start.2 = (bf16[512,256]{1,0:T(8,128)(2,1)S(1)}, bf16[512,256]{1,0:T(8,128)(2,1)S(1)}, u32[]{:S(2)}, u32[]{:S(2)}) collective-permute-start(bf16[512,256]{1,0:T(8,128)(2,1)S(1)} %get-tuple-element.257), channel_id=1, source_target_pairs={{0,8},{8,16},{16,24},{24,32},{32,40},{40,48},{48,56},{56,64},{64,7... | collective-permute-start | bytes 786440 | tf_op jit(solution)/shard_map/ppermute | solution.py:68
  152.4 0.7 copy-start.11
  153.1 1.0 copy-start.3
  153.1 1.0 copy-start.4
  154.0 0.6 copy-start.9
  168.3 15.3 %all-to-all-start.2 = ((bf16[4,384,256]{2,1,0:T(8,128)(2,1)}), bf16[4,384,256]{2,1,0:T(8,128)(2,1)S(1)}, u32[]{:S(2)}, u32[]{:S(2)}) async-start(bf16[4,384,256]{2,1,0:T(8,128)(2,1)} %fusion.11), calls=%async_computation.2 | async-start | bytes 1572864 | tf_op jit(solution)/shard_map/all_to_all | solution.py:51
  204.4 0.7 copy-start.8
  248.2 23.4 %collective-permute-start.5 = (bf16[4,384,256]{2,1,0:T(8,128)(2,1)S(1)}, bf16[4,384,256]{2,1,0:T(8,128)(2,1)S(1)}, u32[]{:S(2)}, u32[]{:S(2)}) collective-permute-start(bf16[4,384,256]{2,1,0:T(8,128)(2,1)S(1)} %get-tuple-element.142), channel_id=1, source_target_pairs={{0,1},{1,0},{2,3},{3,2},{4,5},{5,4},{6,7},{7,6},{8,9},{9,8},{10,11... | collective-permute-start | bytes 2359304 | tf_op jit(solution)/shard_map/ppermute | solution.py:355
Sparse Core Ops, SparseCore 0:
  121.9 120.9 all-gather.1
where the time goes:
time: 296 us; the launch traced here: 295 us
  blocking collectives  128 us (43%)
  waiting for transfers between devices  67.2 us (23%)
  starting transfers between devices  55.1 us (19%)
  between operations  14.2 us (5%)
  other arithmetic  9.74 us (3%)
  local copies, waits for them, and re-layouts  8.5 us (3%)
  Pallas kernels  6.08 us (2%)
  matrix products  5.89 us (2%)
    all_gather x1, blocking collectives, gathered_by_pairs(): lax.all_gather(mine, 'fs', axis=0, tiled=True, axis_index_groups=parity_r...  74.5 us
    all_gather x1, waiting for transfers between devices, on_device(): packed = lax.all_gather(packed, 'fs', axis=0, tiled=True)  37.4 us
    all_gather x2, blocking collectives, gathered_features(): chips = lax.all_gather(shard, 'tp', axis=0, axis_index_groups=chip_rings())  22.1 us
    ppermute x1, starting transfers between devices, on_device(): theirs = lax.ppermute(other, 'tp', [(i, i ^ 1) for i in range(peers)])  21.5 us
    all_to_all x1, blocking collectives, sum_over_chips(): lax.all_to_all(chip_sum, 'tp', 0, 0, tiled=True, axis_index_groups=chip_r...  15.8 us
    all_to_all x1, starting transfers between devices, gathered_features(): lax.all_to_all(both, 'tp', 0, 0, tiled=True, axis_index_groups=core_pairs())  15.4 us
    all_to_all x1, waiting for transfers between devices, sum_over_chips(): lax.all_to_all(chip_sum, 'tp', 0, 0, tiled=True, axis_index_groups=chip_r...  11.7 us
    all_to_all x1, blocking collectives, gathered_features(): lax.all_to_all(both, 'tp', 0, 0, tiled=True, axis_index_groups=core_pairs())  9.13 us
  transfers between devices with their start and end apart: 9, of which 6 were waited for; matrix products, arithmetic and copies ran while one was open for 6% of the time, Pallas kernels for 0%

commit v1 on v0

--- a/solution.py
+++ b/solution.py
@@ -215,17 +215,18 @@
     units = hidden_ref.shape[1]
     blocks, depth = upper_ref.shape[0], upper_ref.shape[1]
     chips, width = down_ref.shape[0], down_ref.shape[1]
-    core = core_ref[0]
+    core, here = core_ref[0], core_ref[1]
+    order = [lax.rem(here + ahead, chips) for ahead in range(chips)]
     upper, down, own = [], [], []
     for k in range(blocks):
         source = packed_ref.at[pl.ds(k * depth, depth), pl.ds(0, 2 * units)]
         upper.append(pltpu.make_async_copy(source, upper_ref.at[k], upper_sem.at[k]))
     for chip in range(chips):
-        rows = pl.ds((2 * chip + 1 - core) * width, width)
+        rows = pl.ds((2 * order[chip] + 1 - core) * width, width)
         source = packed_ref.at[rows, pl.ds(2 * units, units)]
         down.append(pltpu.make_async_copy(source, down_ref.at[chip], down_sem.at[chip]))
     for chip in range(chips):
-        rows = pl.ds((2 * chip + core) * width, width)
+        rows = pl.ds((2 * order[chip] + core) * width, width)
         source = packed_ref.at[rows, pl.ds(2 * units, units)]
         own.append(pltpu.make_async_copy(source, own_down_ref.at[chip], own_sem.at[chip]))
     for copy in upper + down + own:
@@ -350,11 +351,17 @@
     middle = (local.astype(jnp.float32) + merged).astype(jnp.bfloat16)
     normed_mid = rms_scale(gathered_features(middle), middle_gain)
     peers = lax.axis_size("tp")
-    core = (lax.axis_index("tp") % 2).astype(jnp.int32).reshape(1)
+    place = lax.axis_index("tp").astype(jnp.int32)
+    core = jnp.stack([place % 2, place // 2])
     other, hidden, own_down = feed_forward(normed_mid, packed, core, peers)
     theirs = lax.ppermute(other, "tp", [(i, i ^ 1) for i in range(peers)])
     mine = own_share(hidden, own_down)
-    summed = sum_over_chips(mine, theirs)
+    chip_sum = (mine.astype(jnp.float32) + theirs.astype(jnp.float32)).astype(jnp.bfloat16)
+    summed = chip_sum[0].astype(jnp.float32)
+    for ahead in (2, 1, 3):
+        steps = [(i, (i + 2 * ahead) % peers) for i in range(peers)]
+        arrived = lax.ppermute(chip_sum[ahead], "tp", steps)
+        summed = summed + arrived.astype(jnp.float32)
     layer_out = (middle.astype(jnp.float32) + summed).astype(jnp.bfloat16)
     return layer_out.reshape(seq_count, length, part_width)
 

time: 296 us -> 297 us (level)
  blocking collectives: 128 us -> 113 us
  starting transfers between devices: 55.1 us -> 67.3 us
    all_to_all x1 -> x0, blocking collectives: 15.8 us -> none  [sum_over_chips(): lax.all_to_all(chip_sum, 'tp', 0, 0, tiled=True, axis_index_groups=chip_r...]
    ppermute x0 -> x3, starting transfers between devices: none -> 11.2 us  [on_device(): arrived = lax.ppermute(chip_sum[ahead], 'tp', steps)]
    ppermute x0 -> x3, waiting for transfers between devices: none -> 3.29 us  [on_device(): arrived = lax.ppermute(chip_sum[ahead], 'tp', steps)]
  transfers between devices with their start and end apart: 9 -> 12, of which waited for: 6 -> 8; matrix products, arithmetic and copies ran while one was open for 6% -> 6% of each run, Pallas kernels for 0% -> 0%
where the time goes in v1:
time: 297 us; the launch traced here: 295 us
  blocking collectives  113 us (38%)
  waiting for transfers between devices  70 us (24%)
  starting transfers between devices  67.3 us (23%)
  between operations  14.2 us (5%)
  other arithmetic  9.8 us (3%)
  local copies, waits for them, and re-layouts  8.01 us (3%)
  Pallas kernels  6.6 us (2%)
  matrix products  6.46 us (2%)
    all_gather x1, blocking collectives, gathered_by_pairs(): lax.all_gather(mine, 'fs', axis=0, tiled=True, axis_index_groups=parity_r...  74.5 us
    all_gather x1, waiting for transfers between devices, on_device(): packed = lax.all_gather(packed, 'fs', axis=0, tiled=True)  36.9 us
    ppermute x1, starting transfers between devices, on_device(): theirs = lax.ppermute(other, 'tp', [(i, i ^ 1) for i in range(peers)])  22.6 us
    all_gather x2, blocking collectives, gathered_features(): chips = lax.all_gather(shard, 'tp', axis=0, axis_index_groups=chip_rings())  22.4 us
    all_to_all x1, starting transfers between devices, gathered_features(): lax.all_to_all(both, 'tp', 0, 0, tiled=True, axis_index_groups=core_pairs())  15.4 us
    all_to_all x1, waiting for transfers between devices, sum_over_chips(): lax.all_to_all(chip_sum, 'tp', 0, 0, tiled=True, axis_index_groups=chip_r...  11.6 us
    ppermute x3, starting transfers between devices, on_device(): arrived = lax.ppermute(chip_sum[ahead], 'tp', steps)  11.2 us
    all_to_all x1, blocking collectives, gathered_features(): lax.all_to_all(both, 'tp', 0, 0, tiled=True, axis_index_groups=core_pairs())  8.91 us
  transfers between devices with their start and end apart: 12, of which 8 were waited for; matrix products, arithmetic and copies ran while one was open for 6% of the time, Pallas kernels for 0%

profile of v1, /device:TPU:33, one launch (start us, length us, event | category | flops | bytes accessed | tf_op | source)
XLA Modules:
  0.0 295.3 jit_solution(4596965684476560447)
XLA Ops:
  6.5 0.8 maximum_select_fusion
  7.4 0.7 pad_maximum_fusion.5
  8.1 74.5 %all_gather.14 = bf16[1024,384]{1,0:T(8,128)(2,1)S(1)} all-gather(bf16[64,384]{1,0:T(8,128)(2,1)S(1)} %pad_maximum_fusion.5), channel_id=1, replica_groups={{0,16,32,48,64,80,96,112,128,144,160,176,192,208,224,240},{8,24,40,56,7..., dimensions={0}, use_global_device_ids=true | all-gather | bytes 835584 | tf_op jit(solution)/shard_map/all_gather | solution.py:91
  82.6 1.0 fusion.69
  83.5 3.5 %collective-permute-start.3 = (bf16[512,384]{1,0:T(8,128)(2,1)}, bf16[512,384]{1,0:T(8,128)(2,1)}, u32[]{:S(2)}, u32[]{:S(2)}) collective-permute-start(bf16[512,384]{1,0:T(8,128)(2,1)} %get-tuple-element.259), channel_id=1, source_target_pairs={{0,248},{8,0},{16,8},{24,16},{32,24},{40,32},{48,40},{56,48},{64,5... | collective-permute-start | bytes 1179656 | tf_op jit(solution)/shard_map/ppermute | solution.py:67
  87.0 2.0 collective-permute-start.4
  89.0 10.9 %all_gather.13 = bf16[4,384,256]{2,1,0:T(8,128)(2,1)S(1)} all-gather(bf16[1,384,256]{2,1,0:T(8,128)(2,1)S(1)} %copy-done.2), channel_id=1, replica_groups={{0,2,4,6},{1,3,5,7},{8,10,12,14},{9,11,13,15},{16,18,20,22},{17,19,21,2..., dimensions={0}, use_global_device_ids=true | all-gather | bytes 983040 | tf_op jit(solution)/shard_map/all_gather | solution.py:29
  99.9 1.3 broadcast_in_dim.28
  101.2 15.4 %all-to-all-start = ((bf16[2,4,384,256]{3,2,1,0:T(8,128)(2,1)}), bf16[2,4,384,256]{3,2,1,0:T(8,128)(2,1)S(1)}, u32[]{:S(2)}, u32[]{:S(2)}) async-start(bf16[2,4,384,256]{3,2,1,0:T(8,128)(2,1)} %broadcast_in_dim.28), calls=%async_computation | async-start | bytes 3145728 | tf_op jit(solution)/shard_map/all_to_all | solution.py:31
  116.6 0.8 slice.188
  117.4 3.5 %collective-permute-start = (bf16[1024,256]{1,0:T(8,128)(2,1)}, bf16[1024,256]{1,0:T(8,128)(2,1)S(1)}, u32[]{:S(2)}, u32[]{:S(2)}) collective-permute-start(bf16[1024,256]{1,0:T(8,128)(2,1)} %slice.188), channel_id=1, source_target_pairs={{0,256},{256,0},{1,257},{257,1},{2,258},{258,2},{3,259},{259,3},{4... | collective-permute-start | bytes 1572872 | tf_op jit(solution)/shard_map/ppermute | solution.py:92
  121.0 0.7 pad_maximum_fusion.3
  122.0 1.2 copy-done
  123.7 0.6 multiply_exponential_fusion
  124.3 0.6 multiply_exponential_fusion.1
  124.9 0.9 fusion.59
  126.1 1.0 constant_dynamic-update-slice_fusion.3
  127.1 1.1 constant_dynamic-update-slice_fusion.2
  128.5 4.7 %collective-permute-done = bf16[1024,256]{1,0:T(8,128)(2,1)S(1)} collective-permute-done((bf16[1024,256]{1,0:T(8,128)(2,1)}, bf16[1024,256]{1,0:T(8,128)(2,1)S(1)}, u32[]{:S(2)}, u32[]{:S(2)}) %collective-permute-start) | collective-permute-done | bytes 524320 | tf_op jit(solution)/shard_map/ppermute | solution.py:92
  133.3 3.1 %collective-permute-start.1 = (bf16[512,256]{1,0:T(8,128)(2,1)S(1)}, bf16[512,256]{1,0:T(8,128)(2,1)S(1)}, u32[]{:S(2)}, u32[]{:S(2)}) collective-permute-start(bf16[512,256]{1,0:T(8,128)(2,1)S(1)} %get-tuple-element.261), channel_id=1, source_target_pairs={{0,248},{8,0},{16,8},{24,16},{32,24},{40,32},{48,40},{56,48},{64,5... | collective-permute-start | bytes 786440 | tf_op jit(solution)/shard_map/ppermute | solution.py:67
  136.4 2.5 collective-permute-start.2
  138.9 0.9 convolution_convert_fusion.1
  139.8 7.5 %collective-permute-done.1 = bf16[512,256]{1,0:T(8,128)(2,1)S(1)} collective-permute-done((bf16[512,256]{1,0:T(8,128)(2,1)S(1)}, bf16[512,256]{1,0:T(8,128)(2,1)S(1)}, u32[]{:S(2)}, u32[]{:S(2)}) %collective-permute-start.1) | collective-permute-done | bytes 262176 | tf_op jit(solution)/shard_map/ppermute | solution.py:67
  147.3 4.9 %collective-permute-done.2 = bf16[512,256]{1,0:T(8,128)(2,1)S(1)} collective-permute-done((bf16[512,256]{1,0:T(8,128)(2,1)S(1)}, bf16[512,256]{1,0:T(8,128)(2,1)S(1)}, u32[]{:S(2)}, u32[]{:S(2)}) %collective-permute-start.2) | collective-permute-done | bytes 262176 | tf_op jit(solution)/shard_map/ppermute | solution.py:68
  152.5 0.9 broadcast_select_fusion.5
  154.1 0.9 convolution_bitcast_fusion.4
  155.0 0.9 convolution_bitcast_fusion.3
  156.2 0.5 fusion.8
  157.1 0.5 fusion.9
  157.6 0.8 convolution_multiply_fusion
  158.4 0.5 fusion.72
  159.2 0.6 convolution_convert_fusion
  160.3 7.0 %all_to_all.20 = bf16[2,4,384,256]{3,2,1,0:T(8,128)(2,1)S(1)} all-to-all(bf16[2,4,384,256]{3,2,1,0:T(8,128)(2,1)S(1)} %pad_maximum_fusion.1), channel_id=1, replica_groups={{0,1},{2,3},{4,5},{6,7},{8,9},{10,11},{12,13},{14,15},{16,17},{18,19},{..., dimensions={0} | all-to-all | bytes 3145728 | tf_op jit(solution)/shard_map/all_to_all | solution.py:45
  167.3 1.1 fusion.11
  168.4 3.6 %all-to-all-start.2 = ((bf16[4,384,256]{2,1,0:T(8,128)(2,1)}), bf16[4,384,256]{2,1,0:T(8,128)(2,1)S(1)}, u32[]{:S(2)}, u32[]{:S(2)}) async-start(bf16[4,384,256]{2,1,0:T(8,128)(2,1)} %fusion.11), calls=%async_computation.2 | async-start | bytes 1572864 | tf_op jit(solution)/shard_map/all_to_all | solution.py:51
  172.1 11.6 %all-to-all-done.2 = bf16[4,384,256]{2,1,0:T(8,128)(2,1)S(1)} async-done(((bf16[4,384,256]{2,1,0:T(8,128)(2,1)}), bf16[4,384,256]{2,1,0:T(8,128)(2,1)S(1)}, u32[]{:S(2)}, u32[]{:S(2)}) %all-to-all-start.2) | async-done | bytes 786464 | tf_op jit(solution)/shard_map/all_to_all | solution.py:51
  183.9 11.6 %all_gather.15 = bf16[4,384,256]{2,1,0:T(8,128)(2,1)S(1)} all-gather(bf16[1,384,256]{2,1,0:T(8,128)(2,1)S(1)} %fusion.17), channel_id=1, replica_groups={{0,2,4,6},{1,3,5,7},{8,10,12,14},{9,11,13,15},{16,18,20,22},{17,19,21,2..., dimensions={0}, use_global_device_ids=true | all-gather | bytes 983040 | tf_op jit(solution)/shard_map/all_gather | solution.py:29
  195.5 8.9 %all_to_all.21 = bf16[2,4,384,256]{3,2,1,0:T(8,128)(2,1)S(1)} all-to-all(bf16[2,4,384,256]{3,2,1,0:T(8,128)(2,1)S(1)} %broadcast_in_dim.33), channel_id=1, replica_groups={{0,1},{2,3},{4,5},{6,7},{8,9},{10,11},{12,13},{14,15},{16,17},{18,19},{..., dimensions={0} | all-to-all | bytes 3145728 | tf_op jit(solution)/shard_map/all_to_all | solution.py:31
  205.7 36.9 %all-gather.2.cloned.1.call-done.packed_ref = bf16[2048,1920]{1,0:T(8,128)(2,1)} async-done(((bf16[64,1920]{1,0:T(8,128)(2,1)}), bf16[2048,1920]{1,0:T(8,128)(2,1)}) %all-gather.2.cloned.1.call-update) | async-done | bytes 7864336 | tf_op jit(solution)/shard_map/all_gather | solution.py:320
  242.6 5.8 %shard_map.127 = (bf16[4,384,256]{2,1,0:T(8,128)(2,1)S(1)}, bf16[384,640]{1,0:T(8,128)(2,1)S(1)}, bf16[4,256,640]{2,1,0:T(8,128)(2,1)S(1)}) custom-call(s32[2]{0:T(128)S(1)} %pad_add_fusion.core_ref, bf16[384,2048]{1,0:T(8,128)(2,1)S(1)} %fusion.5.normed_ref, bf16[2048,1920]{1,0:T(8,128)(2,1)} %all-gather.2.cloned.1.call-done.packed_ref), custom_call_target="tpu_custom_call" | custom-call | tf_op jit(solution)/shard_map/pallas_call | solution.py:265
  248.4 22.6 %collective-permute-start.5 = (bf16[4,384,256]{2,1,0:T(8,128)(2,1)S(1)}, bf16[4,384,256]{2,1,0:T(8,128)(2,1)S(1)}, u32[]{:S(2)}, u32[]{:S(2)}) collective-permute-start(bf16[4,384,256]{2,1,0:T(8,128)(2,1)S(1)} %get-tuple-element.142), channel_id=1, source_target_pairs={{0,1},{1,0},{2,3},{3,2},{4,5},{5,4},{6,7},{7,6},{8,9},{9,8},{10,11... | collective-permute-start | bytes 2359304 | tf_op jit(solution)/shard_map/ppermute | solution.py:357
  270.9 0.8 shard_map.128
  271.8 1.1 collective-permute-done.5
  273.1 4.6 %collective-permute-start.6 = (bf16[384,256]{1,0:T(8,128)(2,1)S(1)}, bf16[384,256]{1,0:T(8,128)(2,1)S(1)}, u32[]{:S(2)}, u32[]{:S(2)}) collective-permute-start(bf16[384,256]{1,0:T(8,128)(2,1)S(1)} %get-tuple-element.255), channel_id=1, source_target_pairs={{0,4},{1,5},{2,6},{3,7},{4,0},{5,1},{6,2},{7,3},{8,12},{9,13},{10,... | collective-permute-start | bytes 589832 | tf_op jit(solution)/shard_map/ppermute | solution.py:363
  277.7 2.3 collective-permute-start.7
  280.0 4.3 %collective-permute-start.8 = (bf16[384,256]{1,0:T(8,128)(2,1)S(1)}, bf16[384,256]{1,0:T(8,128)(2,1)S(1)}, u32[]{:S(2)}, u32[]{:S(2)}) collective-permute-start(bf16[384,256]{1,0:T(8,128)(2,1)S(1)} %get-tuple-element.256), channel_id=1, source_target_pairs={{0,6},{1,7},{2,0},{3,1},{4,2},{5,3},{6,4},{7,5},{8,14},{9,15},{10,... | collective-permute-start | bytes 589832 | tf_op jit(solution)/shard_map/ppermute | solution.py:363
  284.3 2.9 collective-permute-done.7
  287.6 0.8 fusion.26
  (114 shorter events, 6.1 us)
Async XLA Ops:
  6.5 82.4 %copy-start.2 = (bf16[1,384,256]{2,1,0:T(8,128)(2,1)S(1)}, bf16[1,384,256]{2,1,0:T(8,128)(2,1)}, u32[]{:S(2)}) copy-start(bf16[1,384,256]{2,1,0:T(8,128)(2,1)} %param.17) | copy-start | bytes 589828
  83.5 42.5 %collective-permute-start.3 = (bf16[512,384]{1,0:T(8,128)(2,1)}, bf16[512,384]{1,0:T(8,128)(2,1)}, u32[]{:S(2)}, u32[]{:S(2)}) collective-permute-start(bf16[512,384]{1,0:T(8,128)(2,1)} %get-tuple-element.259), channel_id=1, source_target_pairs={{0,248},{8,0},{16,8},{24,16},{32,24},{40,32},{48,40},{56,48},{64,5... | collective-permute-start | bytes 1179656 | tf_op jit(solution)/shard_map/ppermute | solution.py:67
  87.0 40.1 %collective-permute-start.4 = (bf16[512,384]{1,0:T(8,128)(2,1)}, bf16[512,384]{1,0:T(8,128)(2,1)}, u32[]{:S(2)}, u32[]{:S(2)}) collective-permute-start(bf16[512,384]{1,0:T(8,128)(2,1)} %get-tuple-element.258), channel_id=1, source_target_pairs={{0,8},{8,16},{16,24},{24,32},{32,40},{40,48},{48,56},{56,64},{64,7... | collective-permute-start | bytes 1179656 | tf_op jit(solution)/shard_map/ppermute | solution.py:68
  101.2 19.7 %copy-start.7 = (bf16[640,64]{0,1:T(8,128)(2,1)S(1)}, bf16[640,64]{0,1:T(8,128)(2,1)}, u32[]{:S(2)}) copy-start(bf16[640,64]{0,1:T(8,128)(2,1)} %param.29) | copy-start | bytes 245764
  101.2 19.8 %copy-start.8 = (bf16[64,640]{1,0:T(8,128)(2,1)S(1)}, bf16[64,640]{1,0:T(8,128)(2,1)}, u32[]{:S(2)}) copy-start(bf16[64,640]{1,0:T(8,128)(2,1)} %param.28) | copy-start | bytes 245764
  101.2 19.8 %copy-start.9 = (bf16[64,640]{1,0:T(8,128)(2,1)S(1)}, bf16[64,640]{1,0:T(8,128)(2,1)}, u32[]{:S(2)}) copy-start(bf16[64,640]{1,0:T(8,128)(2,1)} %param.27) | copy-start | bytes 245764
  101.2 20.6 %all-to-all-start = ((bf16[2,4,384,256]{3,2,1,0:T(8,128)(2,1)}), bf16[2,4,384,256]{3,2,1,0:T(8,128)(2,1)S(1)}, u32[]{:S(2)}, u32[]{:S(2)}) async-start(bf16[2,4,384,256]{3,2,1,0:T(8,128)(2,1)} %broadcast_in_dim.28), calls=%async_computation | async-start | bytes 3145728 | tf_op jit(solution)/shard_map/all_to_all | solution.py:31
  116.6 126.0 %all-gather.2.cloned.1.call-start = ((), (), s32[]{:S(2)}) async-start(), calls=%async_computation.4 | async-start | bytes 8110080 | tf_op jit(solution)/shard_map/all_gather | solution.py:320
  117.4 15.8 %collective-permute-start = (bf16[1024,256]{1,0:T(8,128)(2,1)}, bf16[1024,256]{1,0:T(8,128)(2,1)S(1)}, u32[]{:S(2)}, u32[]{:S(2)}) collective-permute-start(bf16[1024,256]{1,0:T(8,128)(2,1)} %slice.188), channel_id=1, source_target_pairs={{0,256},{256,0},{1,257},{257,1},{2,258},{258,2},{3,259},{259,3},{4... | collective-permute-start | bytes 1572872 | tf_op jit(solution)/shard_map/ppermute | solution.py:92
  121.9 1.8 copy-start.11
  121.9 1.8 copy-start.12
  122.0 1.2 copy-start
  128.3 10.6 %copy-start.1 = (bf16[384,2048]{1,0:T(8,128)(2,1)S(1)}, bf16[384,2048]{1,0:T(8,128)(2,1)}, u32[]{:S(2)}) copy-start(bf16[384,2048]{1,0:T(8,128)(2,1)} %copy-done) | copy-start | bytes 4718596
  128.3 10.6 %copy-start.13 = (f32[2048]{0:T(1024)S(1)}, f32[2048]{0:T(1024)}, u32[]{:S(2)}) copy-start(f32[2048]{0:T(1024)} %param.18) | copy-start | bytes 24580
  133.3 14.0 %collective-permute-start.1 = (bf16[512,256]{1,0:T(8,128)(2,1)S(1)}, bf16[512,256]{1,0:T(8,128)(2,1)S(1)}, u32[]{:S(2)}, u32[]{:S(2)}) collective-permute-start(bf16[512,256]{1,0:T(8,128)(2,1)S(1)} %get-tuple-element.261), channel_id=1, source_target_pairs={{0,248},{8,0},{16,8},{24,16},{32,24},{40,32},{48,40},{56,48},{64,5... | collective-permute-start | bytes 786440 | tf_op jit(solution)/shard_map/ppermute | solution.py:67
  136.4 15.8 %collective-permute-start.2 = (bf16[512,256]{1,0:T(8,128)(2,1)S(1)}, bf16[512,256]{1,0:T(8,128)(2,1)S(1)}, u32[]{:S(2)}, u32[]{:S(2)}) collective-permute-start(bf16[512,256]{1,0:T(8,128)(2,1)S(1)} %get-tuple-element.260), channel_id=1, source_target_pairs={{0,8},{8,16},{16,24},{24,32},{32,40},{40,48},{48,56},{56,64},{64,7... | collective-permute-start | bytes 786440 | tf_op jit(solution)/shard_map/ppermute | solution.py:68
  152.4 1.0 copy-start.5
  152.4 1.0 copy-start.6
  153.3 0.7 copy-start.3
  157.1 2.0 copy-start.4
  168.4 15.3 %all-to-all-start.2 = ((bf16[4,384,256]{2,1,0:T(8,128)(2,1)}), bf16[4,384,256]{2,1,0:T(8,128)(2,1)S(1)}, u32[]{:S(2)}, u32[]{:S(2)}) async-start(bf16[4,384,256]{2,1,0:T(8,128)(2,1)} %fusion.11), calls=%async_computation.2 | async-start | bytes 1572864 | tf_op jit(solution)/shard_map/all_to_all | solution.py:51
  204.5 0.7 copy-start.10
  248.4 24.5 %collective-permute-start.5 = (bf16[4,384,256]{2,1,0:T(8,128)(2,1)S(1)}, bf16[4,384,256]{2,1,0:T(8,128)(2,1)S(1)}, u32[]{:S(2)}, u32[]{:S(2)}) collective-permute-start(bf16[4,384,256]{2,1,0:T(8,128)(2,1)S(1)} %get-tuple-element.142), channel_id=1, source_target_pairs={{0,1},{1,0},{2,3},{3,2},{4,5},{5,4},{6,7},{7,6},{8,9},{9,8},{10,11... | collective-permute-start | bytes 2359304 | tf_op jit(solution)/shard_map/ppermute | solution.py:357
  273.1 11.2 %collective-permute-start.6 = (bf16[384,256]{1,0:T(8,128)(2,1)S(1)}, bf16[384,256]{1,0:T(8,128)(2,1)S(1)}, u32[]{:S(2)}, u32[]{:S(2)}) collective-permute-start(bf16[384,256]{1,0:T(8,128)(2,1)S(1)} %get-tuple-element.255), channel_id=1, source_target_pairs={{0,4},{1,5},{2,6},{3,7},{4,0},{5,1},{6,2},{7,3},{8,12},{9,13},{10,... | collective-permute-start | bytes 589832 | tf_op jit(solution)/shard_map/ppermute | solution.py:363
  277.7 9.5 %collective-permute-start.7 = (bf16[384,256]{1,0:T(8,128)(2,1)S(1)}, bf16[384,256]{1,0:T(8,128)(2,1)S(1)}, u32[]{:S(2)}, u32[]{:S(2)}) collective-permute-start(bf16[384,256]{1,0:T(8,128)(2,1)S(1)} %get-tuple-element.257), channel_id=1, source_target_pairs={{0,2},{1,3},{2,4},{3,5},{4,6},{5,7},{6,0},{7,1},{8,10},{9,11},{10,... | collective-permute-start | bytes 589832 | tf_op jit(solution)/shard_map/ppermute | solution.py:363
  280.0 7.6 %collective-permute-start.8 = (bf16[384,256]{1,0:T(8,128)(2,1)S(1)}, bf16[384,256]{1,0:T(8,128)(2,1)S(1)}, u32[]{:S(2)}, u32[]{:S(2)}) collective-permute-start(bf16[384,256]{1,0:T(8,128)(2,1)S(1)} %get-tuple-element.256), channel_id=1, source_target_pairs={{0,6},{1,7},{2,0},{3,1},{4,2},{5,3},{6,4},{7,5},{8,14},{9,15},{10,... | collective-permute-start | bytes 589832 | tf_op jit(solution)/shard_map/ppermute | solution.py:363
Sparse Core Ops, SparseCore 0:
  121.9 120.6 all-gather.1
